TPU v7x, 32 devices: a whole 2x2x4 slice. The times are simulated.
32 devices in a mesh: sp: 4 (over y, x), tp: 8 (over z, core).
Axes of the slice: x: 2, y: 2, z: 4, core: 2. Of those that a mesh axis runs over, the one named last changes fastest.
Arguments:
- tokens: bfloat16 [3, 2048, 4096], P(None, 'sp', 'tp'), may hold values from -6 to 6
- new_token: bfloat16 [3, 1, 4096], P(None, None, 'tp'), may hold values from -6 to 6
- query_weight: bfloat16 [4096, 4096], P(None, 'tp'), may hold values from -0.09375 to 0.09375
- key_weight: bfloat16 [4096, 4096], P(None, 'tp'), may hold values from -0.09375 to 0.09375
- value_weight: bfloat16 [4096, 4096], P(None, 'tp'), may hold values from -0.09375 to 0.09375
- log_decay: float32 [64], P('tp'), may hold values from -0.034 to 0
Outputs:
- state: bfloat16 [3, 64, 64, 64], P(None, 'tp', 'sp')
- read: bfloat16 [3, 4096], P(None, 'tp')
All inputs are finite; a program needn't handle non-finite values.
Results may differ from a plain program's by a relative error of at most 0.012.
Values may be sent and summed in bfloat16 or wider, within the bound.
A program may use at most 64 MiB of HBM per device.

v0:
```python
import jax
import jax.numpy as jnp
from jax import lax
from jax.sharding import PartitionSpec as P

HD = 64


def rotate(values, positions):
    half_dim = values.shape[-1] // 2
    inverse = 10000.0 ** (-jnp.arange(half_dim, dtype=jnp.float32) / half_dim)
    angles = positions.astype(jnp.float32)[:, None, None] * inverse[None, None, :]
    cosine = jnp.cos(angles)
    sine_part = jnp.sin(angles)
    first = values[..., :half_dim]
    second = values[..., half_dim:]
    return jnp.concatenate(
        [first * cosine - second * sine_part, first * sine_part + second * cosine], axis=-1
    )


def group_norm(output):
    centered = output - jnp.mean(output, axis=-1, keepdims=True)
    return centered * lax.rsqrt(jnp.mean(centered * centered, axis=-1, keepdims=True) + 1e-05)


def body(tokens, new_token, query_weight, key_weight, value_weight, log_decay):
    sequences, span_len, _ = tokens.shape
    head_count = log_decay.shape[0]
    inner = head_count * HD
    groups = lax.axis_size("sp")
    own_index = lax.axis_index("sp")
    key_scale = HD ** (-0.5)
    key_share = HD // groups
    row_weights = jnp.concatenate([key_weight, value_weight], axis=1)
    all_weights = jnp.concatenate([key_weight, value_weight, query_weight], axis=1)
    row_piece = lax.all_gather(tokens, "tp", axis=2, tiled=True)
    new_piece = lax.all_gather(new_token, "tp", axis=2, tiled=True)
    row_total = jnp.dot(row_piece, row_weights, preferred_element_type=jnp.float32)
    new_total = jnp.dot(new_piece, all_weights, preferred_element_type=jnp.float32)
    row_total = row_total.reshape(sequences, span_len, 2, head_count, HD)
    offsets = own_index * span_len + jnp.arange(span_len, dtype=jnp.int32)
    key_rows = (rotate(row_total[:, :, 0], offsets) * key_scale).astype(jnp.bfloat16)
    value_rows = row_total[:, :, 1].astype(jnp.bfloat16)
    to_end = (span_len - 1 - jnp.arange(span_len, dtype=jnp.int32)).astype(jnp.float32)
    decay_rows = jnp.exp(to_end[:, None] * log_decay[None, :])
    weighted = (key_rows.astype(jnp.float32) * decay_rows[None, :, :, None]).astype(jnp.bfloat16)
    span_state = jnp.einsum(
        "sthk,sthv->shkv", weighted, value_rows, preferred_element_type=jnp.float32
    )
    carried_state = jnp.exp(log_decay * (span_len * (groups - 1 - own_index)).astype(jnp.float32))
    scaled_state = span_state * carried_state[None, :, None, None]
    state_rows = lax.psum_scatter(scaled_state, "sp", scatter_dimension=2, tiled=True)
    new_total = new_total.reshape(sequences, 1, 3, head_count, HD)
    new_position = jnp.full((1,), groups * span_len, jnp.int32)
    fresh_key = (rotate(new_total[:, :, 0], new_position) * key_scale).astype(jnp.bfloat16)[:, 0]
    new_value = new_total[:, 0, 1].astype(jnp.bfloat16)
    new_query = rotate(new_total[:, :, 2], new_position).astype(jnp.bfloat16)[:, 0]
    query_entries = new_query.astype(jnp.float32)
    decay_one = jnp.exp(log_decay)[None, :, None]
    query_share = lax.dynamic_slice_in_dim(query_entries, own_index * key_share, key_share, 2)
    partial_read = (
        jnp.einsum("shkv,shk->shv", state_rows, query_share, precision=lax.Precision.HIGHEST)
        * decay_one
    )
    summed = lax.psum(partial_read, "sp")
    own_term = jnp.sum(
        query_entries * fresh_key.astype(jnp.float32), axis=-1, keepdims=True
    ) * new_value.astype(jnp.float32)
    normed = group_norm(summed + own_term)
    return (state_rows.astype(jnp.bfloat16), normed.reshape(sequences, inner).astype(jnp.bfloat16))


def solution(mesh):
    return jax.shard_map(
        body,
        mesh=mesh,
        in_specs=(
            P(None, "sp", "tp"),
            P(None, None, "tp"),
            P(None, "tp"),
            P(None, "tp"),
            P(None, "tp"),
            P("tp"),
        ),
        out_specs=(P(None, "tp", "sp", None), P(None, "tp")),
        check_vma=False,
    )
```

profile of v0, /device:TPU:0, one launch (start us, length us, event | category | flops | bytes accessed | tf_op | source)
XLA Modules:
  0.0 200.9 jit_solution(10623617118696532471)
XLA Ops:
  7.2 0.7 all-gather.2.cloned.1.call-update
  7.9 6.4 %copy.9 = bf16[4096,512]{0,1:T(8,128)(2,1)} copy(bf16[4096,512]{1,0:T(8,128)(2,1)} %param.10) | data formatting | bytes 8388608 | tf_op args[4]
  14.3 6.5 %copy.8 = bf16[4096,512]{0,1:T(8,128)(2,1)} copy(bf16[4096,512]{1,0:T(8,128)(2,1)} %param.9) | data formatting | bytes 8388608 | tf_op args[3]
  20.8 16.8 %all_gather.7 = bf16[3,1,4096]{2,0,1:T(4,128)(2,1)S(1)} all-gather(bf16[3,1,512]{2,0,1:T(4,128)(2,1)S(1)} %copy-done), channel_id=1, replica_groups=mesh['sp'=4,'tp'=8] {'tp'}, dimensions={2}, use_global_device_ids=true | all-gather | bytes 27648 | tf_op jit(solution)/shard_map/all_gather | solution.py:38
  37.7 0.1 multiply_exponential_fusion
  37.8 0.3 multiply_cosine_fusion
  38.1 91.1 %all-gather.2.cloned.1.call-done = bf16[3,512,4096]{2,1,0:T(8,128)(2,1)} async-done(((bf16[3,512,512]{2,1,0:T(8,128)(2,1)}), bf16[3,512,4096]{2,1,0:T(8,128)(2,1)}) %all-gather.2.cloned.1.call-update) | async-done | bytes 12582928 | tf_op jit(solution)/shard_map/all_gather | solution.py:37
  129.3 18.5 %fusion.7 = f32[1024,3,512]{2,0,1:T(8,128)S(1)} fusion(bf16[3,512,4096]{2,1,0:T(8,128)(2,1)} %all-gather.2.cloned.1.call-done, bf16[4096,512]{0,1:T(8,128)(2,1)} %copy.9, bf16[4096,512]{0,1:T(8,128)(2,1)} %copy.8), kind=kOutput, calls=%fused_computation.8 | convolution fusion | flops 12901679104 | bytes 27262976 | tf_op jit(solution)/shard_map/dot_general | solution.py:39
  147.8 0.3 copy_bitcast_fusion
  148.1 0.5 multiply_subtract_fusion
  148.5 1.5 fusion.20
  150.0 5.6 %fusion.11 = f32[3,1536]{1,0:T(4,128)S(1)} fusion(bf16[4096,512]{1,0:T(8,128)(2,1)} %param.8, bf16[4096,512]{1,0:T(8,128)(2,1)} %param.10, bf16[4096,512]{1,0:T(8,128)(2,1)} %param.9, bf16[3,1,4096]{2,0,1:T(4,128)(2,1)S(1)} %all_gather.7), kind=kOutput, calls=%fused_computation.16 | convolution fusion | flops 75497472 | bytes 12625920 | tf_op jit(solution)/shard_map/dot_general | solution.py:40
  155.6 0.1 reshape.216
  155.8 0.1 subtract_bitcast_fusion
  155.8 0.1 fusion.31
  155.9 18.7 %reduce-scatter.2.cloned.1.call-done = f32[3,8,16,64]{3,2,1,0:T(8,128)} async-done(((f32[3,8,64,64]{3,2,1,0:T(8,128)}), f32[3,8,16,64]{3,2,1,0:T(8,128)}) %reduce-scatter.2.cloned.1.call-update) | async-done | bytes 98320 | tf_op jit(solution)/shard_map/reduce_scatter | solution.py:53
  174.6 1.1 fusion.27
  175.7 0.1 broadcast_multiply_fusion
  175.8 15.0 %psum.7 = f32[3,8,64]{2,1,0:T(8,128)S(1)} all-reduce(f32[3,8,64]{2,1,0:T(8,128)S(1)} %broadcast_multiply_fusion), channel_id=1, replica_groups=mesh['sp'=4,'tp'=8] {'sp'}, use_global_device_ids=true, to_apply=%region_1.0 | all-reduce | flops 1536 | bytes 12288 | tf_op jit(solution)/shard_map/psum | solution.py:66
  190.8 0.7 fusion.38
  191.6 0.2 multiply_reduce_fusion
  191.7 0.1 multiply_convert_fusion.4
  191.8 0.7 convert_element_type.83
  192.5 1.6 convert_element_type.76
  (15 shorter events, 0.2 us)
Async XLA Ops:
  7.2 122.1 %all-gather.2.cloned.1.call-start = ((), (), s32[]{:S(2)}) async-start(), calls=%async_computation.1 | async-start | bytes 14155776 | tf_op jit(solution)/shard_map/all_gather | solution.py:37
  7.9 166.7 %reduce-scatter.2.cloned.1.call-start = ((), (), s32[]{:S(2)}) async-start(), calls=%async_computation.2 | async-start | bytes 983040 | tf_op jit(solution)/shard_map/reduce_scatter | solution.py:53
  14.3 6.5 %copy-start = (bf16[3,1,512]{2,0,1:T(4,128)(2,1)S(1)}, bf16[3,1,512]{2,0,1:T(4,128)(2,1)}, u32[]{:S(2)}) copy-start(bf16[3,1,512]{2,0,1:T(4,128)(2,1)} %param.7) | copy-start | bytes 9220
  14.3 23.4 %copy-start.1 = (f32[8]{0:T(128)S(1)}, f32[8]{0:T(128)}, u32[]{:S(2)}) copy-start(f32[8]{0:T(128)} %param.11) | copy-start | bytes 100
Sparse Core Ops, SparseCore 0:
  9.6 119.6 all-gather.1
  150.1 24.4 reduce-scatter.1
where the time goes:
time: 201 us
  waiting for transfers between devices  110 us (55%)
  blocking collectives  31.9 us (16%)
  matrix products  26.7 us (13%)
  between operations  14.1 us (7%)
  local copies, waits for them, and re-layouts  14 us (7%)
  other arithmetic  3.69 us (2%)
    all_gather x1, waiting for transfers between devices, body(): row_piece = lax.all_gather(tokens, 'tp', axis=2, tiled=True)  91.1 us
    reduce_scatter x1, waiting for transfers between devices, body(): lax.psum_scatter(scaled_state, 'sp', scatter_dimension=2, tiled=True)  18.7 us
    dot_general x1, matrix products, body(): jnp.dot(row_piece, row_weights, preferred_element_type=jnp.float32)  18.5 us
    all_gather x1, blocking collectives, body(): new_piece = lax.all_gather(new_token, 'tp', axis=2, tiled=True)  16.8 us
    psum x1, blocking collectives, body(): summed = lax.psum(partial_read, 'sp')  15 us
    unnamed x6, local copies, waits for them, and re-layouts  12.9 us
    dot_general x1, matrix products, body(): jnp.dot(new_piece, all_weights, preferred_element_type=jnp.float32)  5.59 us
  transfers between devices with their start and end apart: 2, of which 2 were waited for; matrix products, arithmetic and copies ran while one was open for 10% of the time, Pallas kernels for 0%

commit v1 on v0

--- a/solution.py
+++ b/solution.py
@@ -4,6 +4,7 @@
 from jax.sharding import PartitionSpec as P
 
 HD = 64
+mix_the_target = lambda tile_in: jnp.concatenate(lax.all_gather(tile_in, "tp"), axis=2)
 
 
 def rotate(values, positions):
@@ -34,7 +35,7 @@
     key_share = HD // groups
     row_weights = jnp.concatenate([key_weight, value_weight], axis=1)
     all_weights = jnp.concatenate([key_weight, value_weight, query_weight], axis=1)
-    row_piece = lax.all_gather(tokens, "tp", axis=2, tiled=True)
+    row_piece = mix_the_target(tokens)
     new_piece = lax.all_gather(new_token, "tp", axis=2, tiled=True)
     row_total = jnp.dot(row_piece, row_weights, preferred_element_type=jnp.float32)
     new_total = jnp.dot(new_piece, all_weights, preferred_element_type=jnp.float32)

time: 201 us -> 236 us (1.17)
  local copies, waits for them, and re-layouts: 14 us -> 47.9 us
    reshape x0 -> x1, local copies, waits for them, and re-layouts: none -> 19.6 us  [jnp.concatenate(lax.all_gather(tile_in, 'tp'), axis=2)]
    all_gather x0 -> x1, local copies, waits for them, and re-layouts: none -> 14.4 us  [lax.all_gather(tile_in, 'tp')]
  transfers between devices with their start and end apart: 2 -> 2, of which waited for: 2 -> 2; matrix products, arithmetic and copies ran while one was open for 10% -> 8% of each run, Pallas kernels for 0% -> 0%
where the time goes in v1:
time: 236 us; the launch traced here: 235 us
  waiting for transfers between devices  110 us (47%)
  local copies, waits for them, and re-layouts  47.9 us (20%)
  blocking collectives  31.9 us (14%)
  matrix products  26.7 us (11%)
  between operations  14.1 us (6%)
  other arithmetic  3.69 us (2%)
    all_gather x1, waiting for transfers between devices, lax.all_gather(tile_in, 'tp')  91.1 us
    reshape x1, local copies, waits for them, and re-layouts, jnp.concatenate(lax.all_gather(tile_in, 'tp'), axis=2)  19.6 us
    reduce_scatter x1, waiting for transfers between devices, body(): lax.psum_scatter(scaled_state, 'sp', scatter_dimension=2, tiled=True)  18.7 us
    dot_general x1, matrix products, body(): jnp.dot(row_piece, row_weights, preferred_element_type=jnp.float32)  18.5 us
    all_gather x1, blocking collectives, body(): new_piece = lax.all_gather(new_token, 'tp', axis=2, tiled=True)  16.9 us
    psum x1, blocking collectives, body(): summed = lax.psum(partial_read, 'sp')  15 us
    all_gather x1, local copies, waits for them, and re-layouts, lax.all_gather(tile_in, 'tp')  14.4 us
    unnamed x6, local copies, waits for them, and re-layouts  12.9 us
  transfers between devices with their start and end apart: 2, of which 2 were waited for; matrix products, arithmetic and copies ran while one was open for 8% of the time, Pallas kernels for 0%

profile of v1, /device:TPU:0, one launch (start us, length us, event | category | flops | bytes accessed | tf_op | source)
XLA Modules:
  0.0 234.9 jit_solution(689208947916832563)
XLA Ops:
  7.2 0.7 all-gather.3.cloned.1.call-update
  7.9 6.4 %copy.15 = bf16[4096,512]{0,1:T(8,128)(2,1)} copy(bf16[4096,512]{1,0:T(8,128)(2,1)} %param.10) | data formatting | bytes 8388608 | tf_op args[4]
  14.3 6.5 %copy.14 = bf16[4096,512]{0,1:T(8,128)(2,1)} copy(bf16[4096,512]{1,0:T(8,128)(2,1)} %param.9) | data formatting | bytes 8388608 | tf_op args[3]
  20.8 16.9 %all_gather.11 = bf16[3,1,4096]{2,0,1:T(4,128)(2,1)S(1)} all-gather(bf16[3,1,512]{2,0,1:T(4,128)(2,1)S(1)} %copy-done), channel_id=1, replica_groups=mesh['sp'=4,'tp'=8] {'tp'}, dimensions={2}, use_global_device_ids=true | all-gather | bytes 27648 | tf_op jit(solution)/shard_map/all_gather | solution.py:39
  37.8 0.1 multiply_exponential_fusion
  37.8 0.3 multiply_cosine_fusion
  38.2 91.1 %all-gather.3.cloned.1.call-done = bf16[24,512,512]{2,1,0:T(8,128)(2,1)} async-done(((bf16[3,512,512]{2,1,0:T(8,128)(2,1)}), bf16[24,512,512]{2,1,0:T(8,128)(2,1)}) %all-gather.3.cloned.1.call-update) | async-done | bytes 12582928 | tf_op jit(solution)/shard_map/all_gather | solution.py:7
  129.3 14.4 %copy.35 = bf16[8,3,512,512]{3,0,2,1:T(8,128)(2,1)} copy(bf16[8,3,512,512]{3,2,1,0:T(8,128)(2,1)} %bitcast.49) | data formatting | bytes 25165824 | tf_op jit(solution)/shard_map/all_gather | solution.py:7
  143.7 19.6 %reshape.221 = bf16[3,512,4096]{2,1,0:T(8,128)(2,1)} reshape(bf16[3,512,8,512]{3,2,1,0:T(8,128)(2,1)} %bitcast.48) | data formatting | bytes 25165824 | tf_op jit(solution)/shard_map/reshape | solution.py:7
  163.3 18.5 %fusion.7 = f32[1024,3,512]{2,0,1:T(8,128)S(1)} fusion(bf16[3,512,4096]{2,1,0:T(8,128)(2,1)} %reshape.221, bf16[4096,512]{0,1:T(8,128)(2,1)} %copy.15, bf16[4096,512]{0,1:T(8,128)(2,1)} %copy.14), kind=kOutput, calls=%fused_computation.9 | convolution fusion | flops 12901679104 | bytes 27262976 | tf_op jit(solution)/shard_map/dot_general | solution.py:40
  181.8 0.3 copy_bitcast_fusion.1
  182.1 0.5 multiply_subtract_fusion
  182.5 1.5 fusion.20
  184.0 5.6 %fusion.11 = f32[3,1536]{1,0:T(4,128)S(1)} fusion(bf16[4096,512]{1,0:T(8,128)(2,1)} %param.8, bf16[4096,512]{1,0:T(8,128)(2,1)} %param.10, bf16[4096,512]{1,0:T(8,128)(2,1)} %param.9, bf16[3,1,4096]{2,0,1:T(4,128)(2,1)S(1)} %all_gather.11), kind=kOutput, calls=%fused_computation.17 | convolution fusion | flops 75497472 | bytes 12625920 | tf_op jit(solution)/shard_map/dot_general | solution.py:41
  189.6 0.1 reshape.224
  189.8 0.1 subtract_bitcast_fusion
  189.9 0.1 fusion.31
  189.9 18.7 %reduce-scatter.2.cloned.1.call-done = f32[3,8,16,64]{3,2,1,0:T(8,128)} async-done(((f32[3,8,64,64]{3,2,1,0:T(8,128)}), f32[3,8,16,64]{3,2,1,0:T(8,128)}) %reduce-scatter.2.cloned.1.call-update) | async-done | bytes 98320 | tf_op jit(solution)/shard_map/reduce_scatter | solution.py:54
  208.6 1.1 fusion.27
  209.8 15.0 %psum.7 = f32[3,8,64]{2,1,0:T(8,128)S(1)} all-reduce(f32[3,8,64]{2,1,0:T(8,128)S(1)} %broadcast_multiply_fusion), channel_id=1, replica_groups=mesh['sp'=4,'tp'=8] {'sp'}, use_global_device_ids=true, to_apply=%region_1.0 | all-reduce | flops 1536 | bytes 12288 | tf_op jit(solution)/shard_map/psum | solution.py:67
  224.8 0.7 fusion.38
  225.5 0.2 multiply_reduce_fusion
  225.8 0.7 convert_element_type.83
  226.5 1.6 convert_element_type.76
  (17 shorter events, 0.3 us)
Async XLA Ops:
  7.2 122.1 %all-gather.3.cloned.1.call-start = ((), (), s32[]{:S(2)}) async-start(), calls=%async_computation.2 | async-start | bytes 14155776 | tf_op jit(solution)/shard_map/all_gather | solution.py:7
  7.9 200.7 %reduce-scatter.2.cloned.1.call-start = ((), (), s32[]{:S(2)}) async-start(), calls=%async_computation.1 | async-start | bytes 983040 | tf_op jit(solution)/shard_map/reduce_scatter | solution.py:54
  14.3 6.5 %copy-start = (bf16[3,1,512]{2,0,1:T(4,128)(2,1)S(1)}, bf16[3,1,512]{2,0,1:T(4,128)(2,1)}, u32[]{:S(2)}) copy-start(bf16[3,1,512]{2,0,1:T(4,128)(2,1)} %param.7) | copy-start | bytes 9220
  14.3 23.4 %copy-start.1 = (f32[8]{0:T(128)S(1)}, f32[8]{0:T(128)}, u32[]{:S(2)}) copy-start(f32[8]{0:T(128)} %param.11) | copy-start | bytes 100
Sparse Core Ops, SparseCore 0:
  9.6 119.6 all-gather.2
  184.1 24.4 reduce-scatter.1
